TPU v7x, 32 devices: a whole 2x2x4 slice. The times are simulated.
32 devices in a mesh: sp: 8 (over z, x), tp: 4 (over y, core).
Axes of the slice: x: 2, y: 2, z: 4, core: 2. Of those that a mesh axis runs over, the one named last changes fastest.
Arguments:
- tokens: bfloat16 [768, 1024], P(('sp', 'tp')), may hold values from -11 to 11, as said below
- doc_ids: int32 [768], P('sp'), may hold values from 0 to 1, never falling along the last dimension, each value on 1 to 576 neighbouring positions
- query_down: bfloat16 [1024, 384], P('sp'), may hold values from -0.1875 to 0.1875
- query_gain: float32 [384], replicated, may hold values from 0.1 to 1.9
- query_up: bfloat16 [384, 16, 96], P('sp', 'tp'), may hold values from -0.3125 to 0.3125
- latent_down: bfloat16 [1024, 256], P('sp'), may hold values from -0.1875 to 0.1875
- latent_gain: float32 [256], replicated, may hold values from 0.1 to 1.9
- rope_down: bfloat16 [1024, 32], P('sp'), may hold values from -0.1875 to 0.1875
- key_up: bfloat16 [256, 16, 64], P('sp', 'tp'), may hold values from -0.375 to 0.375
- value_up: bfloat16 [256, 16, 64], P('sp', 'tp'), may hold values from -0.375 to 0.375
- output_weight: bfloat16 [1024, 1024], P('tp', 'sp'), may hold values from -0.1875 to 0.1875
- output_gain: float32 [1024], replicated, may hold values from 0.1 to 1.9
Outputs:
- layer_out: bfloat16 [768, 1024], P(('sp', 'tp'))
Inputs may be any that keep to these rules, and one draw needn't show every extreme that they name: Every entry of tokens lies between -11 and 11. `doc_ids`: document numbers never fall along the sequence; each document holds 1 to 576 positions.
All inputs are finite; a program needn't handle non-finite values.
Results may differ from a plain program's by a relative error of at most 0.02.
Values may be sent and summed in bfloat16 or wider, within the bound.
A program may use at most 64 MiB of HBM per device.

v0:
```python
import jax
import jax.numpy as jnp
from jax import lax
from jax.sharding import PartitionSpec as P

ROPE_BASE = 10000.0
EPS = 1e-06
MASKED = -1e30


def folded(value, axis, dim, update, carry):
    whole = jax.tree.map(lambda part: lax.all_gather(part, axis, axis=dim, tiled=True), value)
    return update(carry, whole, jnp.int32(0))


def gathered_then(share, axis, dim, apply):
    everything = lax.all_gather(share, axis, axis=dim, tiled=True)
    return apply(everything, jnp.int32(0))


def for_sending(value):

    def short(part):
        return part.astype(jnp.bfloat16) if part.dtype == jnp.float32 else part

    return jax.tree.map(short, value)


def own_rows(term, extent, axis):
    whole = term(jnp.int32(0), extent * lax.axis_size(axis)).astype(jnp.bfloat16)
    return lax.psum_scatter(whole, axis, scatter_dimension=0, tiled=True).astype(jnp.float32)


def normalize(values, gain_vec):
    return values * lax.rsqrt(jnp.mean(values * values, axis=-1, keepdims=True) + EPS) * gain_vec


def rotate(rope_part, position):
    half_width = rope_part.shape[-1] // 2
    frequency = ROPE_BASE ** (
        -jnp.arange(0, 2 * half_width, 2, dtype=jnp.float32) / (2 * half_width)
    )
    angles = position.astype(jnp.float32)[:, None] * frequency[None, :]
    cosine = jnp.cos(angles)
    sine_part = jnp.sin(angles)
    if rope_part.ndim == 3:
        cosine = cosine[:, None, :]
        sine_part = sine_part[:, None, :]
    first_half = rope_part[..., :half_width]
    second_half = rope_part[..., half_width:]
    return jnp.concatenate(
        [
            first_half * cosine - second_half * sine_part,
            first_half * sine_part + second_half * cosine,
        ],
        axis=-1,
    )


def on_device(
    tokens,
    doc_ids,
    query_down,
    query_gain,
    query_up,
    latent_down,
    latent_gain,
    rope_down,
    key_up,
    value_up,
    output_weight,
    output_gain,
):
    row_count = tokens.shape[0]
    key_span = doc_ids.shape[0]
    query_width = query_down.shape[1]
    latent_width = latent_down.shape[1]
    rope_width = rope_down.shape[1]
    local_heads = query_up.shape[1]
    head_width = query_up.shape[2]
    nope_width = key_up.shape[2]
    value_width = value_up.shape[2]

    def down_term(total_now, weight_rows, first_row):
        columns = lax.dynamic_slice_in_dim(tokens, first_row, weight_rows.shape[0], 1)
        return total_now + jnp.dot(columns, weight_rows, preferred_element_type=jnp.float32)

    empty_query = jnp.zeros((row_count, query_width), jnp.float32)
    empty_latent = jnp.zeros((row_count, latent_width), jnp.float32)
    empty_rope = jnp.zeros((row_count, rope_width), jnp.float32)
    query_sum = folded(query_down, "sp", 0, down_term, empty_query)
    latent_sum = folded(latent_down, "sp", 0, down_term, empty_latent)
    rope_sum = folded(rope_down, "sp", 0, down_term, empty_rope)
    query_lat = normalize(query_sum, query_gain).astype(jnp.bfloat16)
    kv_lat = normalize(latent_sum, latent_gain).astype(jnp.bfloat16)
    own_position = lax.axis_index(("sp", "tp")) * row_count + lax.iota(jnp.int32, row_count)
    rope_keys = rotate(rope_sum, own_position).astype(jnp.bfloat16)
    query_full, key_full, value_full = (
        lax.all_gather(query_up, "sp", axis=0, tiled=True),
        lax.all_gather(key_up, "sp", axis=0, tiled=True),
        lax.all_gather(value_up, "sp", axis=0, tiled=True),
    )
    flat_width = local_heads * head_width
    query_matrix = query_full.reshape(query_width, flat_width)
    block_offset = lax.axis_index("sp") * key_span

    def project(latent_rows, first_row):
        piece_rows = latent_rows.shape[0]
        raw_query = jnp.dot(
            latent_rows[:, :query_width], query_matrix, preferred_element_type=jnp.float32
        ).reshape(piece_rows, local_heads, head_width)
        position = block_offset + first_row + lax.iota(jnp.int32, piece_rows)
        turned = jnp.concatenate(
            [raw_query[..., :nope_width], rotate(raw_query[..., nope_width:], position)], axis=-1
        )
        return jnp.concatenate(
            [
                turned.astype(jnp.bfloat16).reshape(piece_rows, flat_width),
                latent_rows[:, query_width:],
            ],
            axis=1,
        )

    packed = jnp.concatenate([query_lat, kv_lat, rope_keys], axis=1)
    gathered = gathered_then(packed, "tp", 0, project)
    queries = gathered[:, :flat_width].reshape(key_span, local_heads, head_width)
    my_ids = doc_ids.astype(jnp.bfloat16)
    key_rows = jnp.concatenate([gathered[:, flat_width:], my_ids[:, None]], axis=1)
    query_nope = queries[..., :nope_width]
    query_rope = queries[..., nope_width:]
    score_scale = head_width ** (-0.5)
    absorbed = jnp.einsum("qhe,rhe->qhr", query_nope, key_full, preferred_element_type=jnp.float32)

    def block_scores(latent_part, rope_part):
        latent_float = latent_part.astype(jnp.float32)
        scores = jnp.einsum("qhr,kr->qhk", absorbed, latent_float, precision=lax.Precision.HIGHEST)
        scores = scores + jnp.einsum(
            "qhe,ke->qhk", query_rope, rope_part, preferred_element_type=jnp.float32
        )
        return (scores * score_scale, latent_float)

    def finish(averaged):
        return jnp.einsum(
            "qhr,rhv->qhv",
            averaged,
            value_full.astype(jnp.float32),
            precision=lax.Precision.HIGHEST,
        )

    def scan_step(state_now, block_keys):
        row_peak, row_total, running = state_now
        latent_part = block_keys[:, :latent_width]
        rope_part = block_keys[:, latent_width : latent_width + rope_width]
        block_ids = block_keys[:, latent_width + rope_width]
        scores, value_part = block_scores(latent_part, rope_part)
        same_doc = my_ids[:, None, None] == block_ids[None, None, :]
        peak_new = jnp.maximum(row_peak, jnp.max(jnp.where(same_doc, scores, MASKED), axis=-1))
        soft_weights = jnp.where(same_doc, jnp.exp(scores - peak_new[..., None]), 0.0)
        factor = jnp.exp(row_peak - peak_new)
        if value_part.ndim == 3:
            contrib = jnp.einsum(
                "qhk,khv->qhv", soft_weights, value_part, precision=lax.Precision.HIGHEST
            )
        else:
            contrib = jnp.einsum(
                "qhk,kv->qhv", soft_weights, value_part, precision=lax.Precision.HIGHEST
            )
        next_state = (
            peak_new,
            row_total * factor + jnp.sum(soft_weights, axis=-1),
            running * factor[..., None] + contrib,
        )
        return (next_state, None)

    def fold_keys(state_now, key_piece, first_row):
        key_blocks = key_piece.reshape(key_piece.shape[0] // key_span, key_span, key_piece.shape[1])
        return lax.scan(scan_step, state_now, key_blocks)[0]

    start_state = (
        jnp.full((key_span, local_heads), MASKED, jnp.float32),
        jnp.zeros((key_span, local_heads), jnp.float32),
        jnp.zeros((key_span, local_heads, latent_width), jnp.float32),
    )
    row_peak, row_total, running = folded(for_sending(key_rows), "sp", 0, fold_keys, start_state)
    averaged = running / row_total[..., None]
    attended = finish(averaged).astype(jnp.bfloat16).reshape(key_span, local_heads * value_width)
    out_full = lax.all_gather(output_weight, "sp", axis=1, tiled=True)

    def out_term(first_row, row_span):
        row_block = lax.dynamic_slice_in_dim(attended, first_row, row_span, 0)
        return jnp.dot(row_block, out_full, preferred_element_type=jnp.float32)

    mixed = own_rows(out_term, row_count, "tp")
    return normalize(mixed, output_gain).astype(jnp.bfloat16)


def solution(mesh):
    in_specs = (
        P(("sp", "tp"), None),
        P("sp"),
        P("sp", None),
        P(),
        P("sp", "tp", None),
        P("sp", None),
        P(),
        P("sp", None),
        P("sp", "tp", None),
        P("sp", "tp", None),
        P("tp", "sp"),
        P(),
    )
    out_specs = P(("sp", "tp"), None)
    return jax.shard_map(
        on_device, mesh=mesh, in_specs=in_specs, out_specs=out_specs, check_vma=False
    )
```

profile of v0, /device:TPU:0, one launch (start us, length us, event | category | flops | bytes accessed | tf_op | source)
XLA Modules:
  0.0 298.6 jit_solution(12510070031708650458)
XLA Ops:
  6.6 28.0 %all_gather.29 = bf16[1024,32]{0,1:T(8,128)(2,1)S(1)} all-gather(bf16[128,32]{0,1:T(8,128)(2,1)} %param.21), channel_id=1, replica_groups=mesh['sp'=8,'tp'=4] {'sp'}, dimensions={0}, use_global_device_ids=true | all-gather | bytes 73728 | tf_op jit(solution)/shard_map/all_gather | solution.py:12
  34.6 32.1 %all_gather.27 = bf16[1024,384]{1,0:T(8,128)(2,1)S(1)} all-gather(bf16[128,384]{1,0:T(8,128)(2,1)S(1)} %copy-done.3), channel_id=1, replica_groups=mesh['sp'=8,'tp'=4] {'sp'}, dimensions={0}, use_global_device_ids=true | all-gather | bytes 884736 | tf_op jit(solution)/shard_map/all_gather | solution.py:12
  67.1 0.5 copy-done.4
  67.6 31.3 %all_gather.28 = bf16[1024,256]{1,0:T(8,128)(2,1)S(1)} all-gather(bf16[128,256]{1,0:T(8,128)(2,1)S(1)} %copy-done.4), channel_id=1, replica_groups=mesh['sp'=8,'tp'=4] {'sp'}, dimensions={0}, use_global_device_ids=true | all-gather | bytes 589824 | tf_op jit(solution)/shard_map/all_gather | solution.py:12
  99.4 0.5 copy-done.10
  100.0 0.7 copy-done.11
  100.8 5.6 %all_gather.30 = bf16[96,672]{1,0:T(8,128)(2,1)S(1)} all-gather(bf16[24,672]{1,0:T(8,128)(2,1)S(1)} %pad_maximum_fusion.1), channel_id=1, replica_groups=mesh['sp'=8,'tp'=4] {'tp'}, dimensions={0}, use_global_device_ids=true | all-gather | bytes 161280 | tf_op jit(solution)/shard_map/all_gather | solution.py:17
  106.4 31.2 %all_gather.32 = bf16[384,4,96]{2,1,0:T(4,128)(2,1)S(1)} all-gather(bf16[48,4,96]{2,1,0:T(4,128)(2,1)S(1)} %copy-done.6), channel_id=1, replica_groups=mesh['sp'=8,'tp'=4] {'sp'}, dimensions={0}, use_global_device_ids=true | all-gather | bytes 331776 | tf_op jit(solution)/shard_map/all_gather | solution.py:99
  138.7 31.0 %all_gather.33 = bf16[256,4,64]{2,0,1:T(8,128)(2,1)S(1)} all-gather(bf16[32,4,64]{2,0,1:T(8,128)(2,1)S(1)} %copy.29), channel_id=1, replica_groups=mesh['sp'=8,'tp'=4] {'sp'}, dimensions={0}, use_global_device_ids=true | all-gather | bytes 147456 | tf_op jit(solution)/shard_map/all_gather | solution.py:100
  169.9 31.4 %all_gather.31 = bf16[768,289]{1,0:T(8,128)(2,1)S(1)} all-gather(bf16[96,289]{1,0:T(8,128)(2,1)S(1)} %pad_maximum_fusion), channel_id=1, replica_groups=mesh['sp'=8,'tp'=4] {'sp'}, dimensions={0}, use_global_device_ids=true | all-gather | bytes 499392 | tf_op jit(solution)/shard_map/all_gather | solution.py:12
  201.6 11.6 %while.15 = (s32[]{:T(128)}, f32[96,4]{0,1:T(4,128)S(1)}, f32[96,4]{0,1:T(4,128)S(1)}, f32[96,4,256]{2,0,1:T(8,128)S(1)}, bf16[96]{0:T(256)(128)(2,1)S(1)}, /*in...) while((s32[]{:T(128)}, f32[96,4]{0,1:T(4,128)S(1)}, ...), condition=%wide.region_5.6_spmd.clone, body=%wide.region_2.5_spmd.clone.sunk | while | flops 229489536 | bytes 2351349 | solution.py:177
  202.1 0.4 select_reduce_fusion.2
  202.6 0.5 convolution_add_fusion.3
  203.5 0.4 select_reduce_fusion.2
  204.0 0.5 convolution_add_fusion.3
  205.0 0.4 select_reduce_fusion.2
  205.5 0.5 convolution_add_fusion.3
  206.4 0.4 select_reduce_fusion.2
  206.9 0.5 convolution_add_fusion.3
  207.9 0.4 select_reduce_fusion.2
  208.4 0.5 convolution_add_fusion.3
  209.3 0.4 select_reduce_fusion.2
  209.8 0.5 convolution_add_fusion.3
  211.3 0.5 convolution_add_fusion.3
  212.7 0.5 convolution_add_fusion.3
  213.3 31.0 %all_gather.34 = bf16[256,4,64]{2,0,1:T(8,128)(2,1)S(1)} all-gather(bf16[32,4,64]{2,0,1:T(8,128)(2,1)S(1)} %copy.30), channel_id=1, replica_groups=mesh['sp'=8,'tp'=4] {'sp'}, dimensions={0}, use_global_device_ids=true | all-gather | bytes 147456 | tf_op jit(solution)/shard_map/all_gather | solution.py:101
  244.3 27.0 %all_gather.35 = bf16[256,1024]{1,0:T(8,128)(2,1)S(1)} all-gather(bf16[256,128]{1,0:T(8,128)(2,1)S(1)} %copy-done.5), channel_id=1, replica_groups=mesh['sp'=8,'tp'=4] {'sp'}, dimensions={1}, use_global_device_ids=true | all-gather | bytes 589824 | tf_op jit(solution)/shard_map/all_gather | solution.py:187
  271.3 0.5 convolution_convert_fusion.1
  271.8 0.9 convolution_convert_fusion
  272.8 17.3 %reduce-scatter.2.cloned.1.call-done = bf16[24,1024]{1,0:T(8,128)(2,1)} async-done(((bf16[96,1024]{1,0:T(8,128)(2,1)}), bf16[24,1024]{1,0:T(8,128)(2,1)}) %reduce-scatter.2.cloned.1.call-update) | async-done | bytes 49168 | tf_op jit(solution)/shard_map/reduce_scatter | solution.py:31
  290.1 1.0 fusion.13
  291.1 0.7 fusion.15
  (120 shorter events, 7.7 us)
Async XLA Ops:
  6.5 60.1 %copy-start = (bf16[24,1024]{1,0:T(8,128)(2,1)S(1)}, bf16[24,1024]{1,0:T(8,128)(2,1)}, u32[]{:S(2)}) copy-start(bf16[24,1024]{1,0:T(8,128)(2,1)} %param.14) | copy-start | bytes 147460
  6.5 28.1 %copy-start.3 = (bf16[128,384]{1,0:T(8,128)(2,1)S(1)}, bf16[128,384]{1,0:T(8,128)(2,1)}, u32[]{:S(2)}) copy-start(bf16[128,384]{1,0:T(8,128)(2,1)} %param.16) | copy-start | bytes 294916
  6.5 283.5 %reduce-scatter.2.cloned.1.call-start = ((), (), s32[]{:S(2)}) async-start(), calls=%async_computation.1 | async-start | bytes 245760 | tf_op jit(solution)/shard_map/reduce_scatter | solution.py:31
  66.8 0.9 copy-start.4
  99.2 0.7 copy-start.10
  100.0 0.7 copy-start.11
  100.8 5.6 %copy-start.6 = (bf16[48,4,96]{2,1,0:T(4,128)(2,1)S(1)}, bf16[48,4,96]{2,1,0:T(4,128)(2,1)}, u32[]{:S(2)}) copy-start(bf16[48,4,96]{2,1,0:T(4,128)(2,1)} %param.18) | copy-start | bytes 110596
  106.4 31.5 %copy-start.1 = (bf16[96,672]{1,0:T(8,128)(2,1)}, bf16[96,672]{1,0:T(8,128)(2,1)S(1)}, u32[]{:S(2)}) copy-start(bf16[96,672]{1,0:T(8,128)(2,1)S(1)} %all_gather.30) | copy-start | bytes 387076
  137.9 0.8 copy-start.7
  138.7 31.0 %copy-start.12 = (s32[96]{0:T(128)S(1)}, s32[96]{0:T(128)}, u32[]{:S(2)}) copy-start(s32[96]{0:T(128)} %param.15) | copy-start | bytes 1156
  138.7 31.2 %slice-start = ((bf16[96,672]{1,0:T(8,128)(2,1)}), bf16[96,288]{1,0:T(8,128)(2,1)S(1)}, s32[]{:S(2)}) async-start(bf16[96,672]{1,0:T(8,128)(2,1)} %copy-done.1), calls=%async_computation.2 | async-start | bytes 147456 | tf_op jit(solution)/shard_map/slice | solution.py:119
  201.6 11.6 %copy-start.8 = (bf16[32,4,64]{2,1,0:T(4,128)(2,1)S(1)}, bf16[32,4,64]{2,1,0:T(4,128)(2,1)}, u32[]{:S(2)}) copy-start(bf16[32,4,64]{2,1,0:T(4,128)(2,1)} %param.23) | copy-start | bytes 49156
  213.2 31.1 %copy-start.5 = (bf16[256,128]{1,0:T(8,128)(2,1)S(1)}, bf16[256,128]{1,0:T(8,128)(2,1)}, u32[]{:S(2)}) copy-start(bf16[256,128]{1,0:T(8,128)(2,1)} %param.24) | copy-start | bytes 196612
  272.7 18.3 %copy-start.9 = (f32[1024]{0:T(1024)S(1)}, f32[1024]{0:T(1024)}, u32[]{:S(2)}) copy-start(f32[1024]{0:T(1024)} %param.25) | copy-start | bytes 12292
  290.1 1.0 copy-start.2
Sparse Core Ops, SparseCore 0:
  272.9 17.1 reduce-scatter.1
where the time goes:
time: 299 us
  blocking collectives  249 us (83%)
  waiting for transfers between devices  17.3 us (6%)
  between operations  13.6 us (5%)
  matrix products  10.7 us (4%)
  local copies, waits for them, and re-layouts  4.08 us (1%)
  other arithmetic  3.78 us (1%)
    all_gather x4, blocking collectives, folded(): lax.all_gather(part, axis, axis=dim, tiled=True)  123 us
    all_gather x1, blocking collectives, on_device(): lax.all_gather(query_up, 'sp', axis=0, tiled=True)  31.2 us
    all_gather x1, blocking collectives, on_device(): lax.all_gather(value_up, 'sp', axis=0, tiled=True)  31 us
    all_gather x1, blocking collectives, on_device(): lax.all_gather(key_up, 'sp', axis=0, tiled=True)  31 us
    all_gather x1, blocking collectives, on_device(): out_full = lax.all_gather(output_weight, 'sp', axis=1, tiled=True)  27 us
    reduce_scatter x1, waiting for transfers between devices, own_rows(): lax.psum_scatter(whole, axis, scatter_dimension=0, tiled=True)  17.3 us
  transfers between devices with their start and end apart: 1, of which 1 were waited for; matrix products, arithmetic and copies ran while one was open for 0% of the time, Pallas kernels for 0%

commit v1 on v0

--- a/solution.py
+++ b/solution.py
@@ -98,7 +98,9 @@
     query_full, key_full, value_full = (
         lax.all_gather(query_up, "sp", axis=0, tiled=True),
         lax.all_gather(key_up, "sp", axis=0, tiled=True),
-        lax.all_gather(value_up, "sp", axis=0, tiled=True),
+        jnp.concatenate(
+            lax.all_to_all(jnp.stack([value_up] * lax.axis_size("sp")), "sp", 0, 0), axis=0
+        ),
     )
     flat_width = local_heads * head_width
     query_matrix = query_full.reshape(query_width, flat_width)

time: 299 us -> 276 us (0.923)
  blocking collectives: 249 us -> 216 us
  starting transfers between devices: 0.01 us -> 7.45 us
    all_gather x1 -> x0, blocking collectives: 31 us -> none  [on_device(): lax.all_gather(value_up, 'sp', axis=0, tiled=True)]
    all_to_all x0 -> x1, starting transfers between devices: none -> 7.41 us  [on_device(): lax.all_to_all(jnp.stack([value_up] * lax.axis_size('sp')), 'sp', 0, 0)]
  transfers between devices with their start and end apart: 1 -> 2, of which waited for: 1 -> 1; matrix products, arithmetic and copies ran while one was open for 0% -> 5% of each run, Pallas kernels for 0% -> 0%
where the time goes in v1:
time: 276 us; the launch traced here: 275 us
  blocking collectives  216 us (78%)
  waiting for transfers between devices  17.5 us (6%)
  between operations  13.7 us (5%)
  matrix products  10.7 us (4%)
  starting transfers between devices  7.45 us (3%)
  local copies, waits for them, and re-layouts  5.69 us (2%)
  other arithmetic  3.79 us (1%)
    all_gather x4, blocking collectives, folded(): lax.all_gather(part, axis, axis=dim, tiled=True)  122 us
    all_gather x1, blocking collectives, on_device(): lax.all_gather(query_up, 'sp', axis=0, tiled=True)  31.1 us
    all_gather x1, blocking collectives, on_device(): lax.all_gather(key_up, 'sp', axis=0, tiled=True)  30.9 us
    all_gather x1, blocking collectives, on_device(): out_full = lax.all_gather(output_weight, 'sp', axis=1, tiled=True)  27 us
    reduce_scatter x1, waiting for transfers between devices, own_rows(): lax.psum_scatter(whole, axis, scatter_dimension=0, tiled=True)  17.5 us
    all_to_all x1, starting transfers between devices, on_device(): lax.all_to_all(jnp.stack([value_up] * lax.axis_size('sp')), 'sp', 0, 0)  7.41 us
    all_gather x1, blocking collectives, gathered_then(): everything = lax.all_gather(share, axis, axis=dim, tiled=True)  5.58 us
  transfers between devices with their start and end apart: 2, of which 1 were waited for; matrix products, arithmetic and copies ran while one was open for 5% of the time, Pallas kernels for 0%

profile of v1, /device:TPU:0, one launch (start us, length us, event | category | flops | bytes accessed | tf_op | source)
XLA Modules:
  0.0 275.5 jit_solution(7167321162988163040)
XLA Ops:
  6.5 0.8 copy.31
  7.4 0.9 reshape.149
  8.2 7.4 %all-to-all-start = ((bf16[8,2,4096]{2,1,0:T(2,128)(2,1)}), bf16[8,2,4096]{2,1,0:T(2,128)(2,1)S(1)}, u32[]{:S(2)}, u32[]{:S(2)}) async-start(bf16[8,2,4096]{2,1,0:T(2,128)(2,1)} %reshape.149), calls=%async_computation | async-start | bytes 262144 | tf_op jit(solution)/shard_map/all_to_all | solution.py:102
  15.8 26.5 %all_gather.26 = bf16[1024,32]{0,1:T(8,128)(2,1)S(1)} all-gather(bf16[128,32]{0,1:T(8,128)(2,1)S(1)} %copy-done.8), channel_id=1, replica_groups=mesh['sp'=8,'tp'=4] {'sp'}, dimensions={0}, use_global_device_ids=true | all-gather | bytes 73728 | tf_op jit(solution)/shard_map/all_gather | solution.py:12
  42.3 32.0 %all_gather.24 = bf16[1024,384]{1,0:T(8,128)(2,1)S(1)} all-gather(bf16[128,384]{1,0:T(8,128)(2,1)S(1)} %copy-done.3), channel_id=1, replica_groups=mesh['sp'=8,'tp'=4] {'sp'}, dimensions={0}, use_global_device_ids=true | all-gather | bytes 884736 | tf_op jit(solution)/shard_map/all_gather | solution.py:12
  74.8 0.5 copy-done.4
  75.3 31.3 %all_gather.25 = bf16[1024,256]{1,0:T(8,128)(2,1)S(1)} all-gather(bf16[128,256]{1,0:T(8,128)(2,1)S(1)} %copy-done.4), channel_id=1, replica_groups=mesh['sp'=8,'tp'=4] {'sp'}, dimensions={0}, use_global_device_ids=true | all-gather | bytes 589824 | tf_op jit(solution)/shard_map/all_gather | solution.py:12
  107.4 0.7 copy-done.11
  108.2 5.6 %all_gather.27 = bf16[96,672]{1,0:T(8,128)(2,1)S(1)} all-gather(bf16[24,672]{1,0:T(8,128)(2,1)S(1)} %pad_maximum_fusion.1), channel_id=1, replica_groups=mesh['sp'=8,'tp'=4] {'tp'}, dimensions={0}, use_global_device_ids=true | all-gather | bytes 161280 | tf_op jit(solution)/shard_map/all_gather | solution.py:17
  113.8 31.1 %all_gather.29 = bf16[384,4,96]{2,1,0:T(4,128)(2,1)S(1)} all-gather(bf16[48,4,96]{2,1,0:T(4,128)(2,1)S(1)} %copy-done.6), channel_id=1, replica_groups=mesh['sp'=8,'tp'=4] {'sp'}, dimensions={0}, use_global_device_ids=true | all-gather | bytes 331776 | tf_op jit(solution)/shard_map/all_gather | solution.py:99
  146.0 30.9 %all_gather.30 = bf16[256,4,64]{2,0,1:T(8,128)(2,1)S(1)} all-gather(bf16[32,4,64]{2,0,1:T(8,128)(2,1)S(1)} %copy.30), channel_id=1, replica_groups=mesh['sp'=8,'tp'=4] {'sp'}, dimensions={0}, use_global_device_ids=true | all-gather | bytes 147456 | tf_op jit(solution)/shard_map/all_gather | solution.py:100
  177.1 31.7 %all_gather.28 = bf16[768,289]{1,0:T(8,128)(2,1)S(1)} all-gather(bf16[96,289]{1,0:T(8,128)(2,1)S(1)} %pad_maximum_fusion), channel_id=1, replica_groups=mesh['sp'=8,'tp'=4] {'sp'}, dimensions={0}, use_global_device_ids=true | all-gather | bytes 499392 | tf_op jit(solution)/shard_map/all_gather | solution.py:12
  209.1 11.6 %while.15 = (s32[]{:T(128)}, f32[96,4]{0,1:T(4,128)S(1)}, f32[96,4]{0,1:T(4,128)S(1)}, f32[96,4,256]{2,0,1:T(8,128)S(1)}, bf16[96]{0:T(256)(128)(2,1)S(1)}, /*in...) while((s32[]{:T(128)}, f32[96,4]{0,1:T(4,128)S(1)}, ...), condition=%wide.region_5.6_spmd.clone, body=%wide.region_2.5_spmd.clone.sunk | while | flops 229489536 | bytes 2351349 | solution.py:179
  209.5 0.4 select_reduce_fusion.2
  210.0 0.5 convolution_add_fusion.3
  211.0 0.4 select_reduce_fusion.2
  211.5 0.5 convolution_add_fusion.3
  212.4 0.4 select_reduce_fusion.2
  212.9 0.5 convolution_add_fusion.3
  214.4 0.5 convolution_add_fusion.3
  215.8 0.5 convolution_add_fusion.3
  217.3 0.5 convolution_add_fusion.3
  218.2 0.4 select_reduce_fusion.2
  218.7 0.5 convolution_add_fusion.3
  219.7 0.4 select_reduce_fusion.2
  220.2 0.5 convolution_add_fusion.3
  220.7 27.0 %all_gather.31 = bf16[256,1024]{1,0:T(8,128)(2,1)S(1)} all-gather(bf16[256,128]{1,0:T(8,128)(2,1)S(1)} %copy-done.5), channel_id=1, replica_groups=mesh['sp'=8,'tp'=4] {'sp'}, dimensions={1}, use_global_device_ids=true | all-gather | bytes 589824 | tf_op jit(solution)/shard_map/all_gather | solution.py:189
  248.0 0.5 convolution_convert_fusion.1
  248.5 0.9 convolution_convert_fusion
  249.4 17.5 %reduce-scatter.2.cloned.1.call-done = bf16[24,1024]{1,0:T(8,128)(2,1)} async-done(((bf16[96,1024]{1,0:T(8,128)(2,1)}), bf16[24,1024]{1,0:T(8,128)(2,1)}) %reduce-scatter.2.cloned.1.call-update) | async-done | bytes 49168 | tf_op jit(solution)/shard_map/reduce_scatter | solution.py:31
  266.9 1.0 fusion.13
  267.9 0.7 fusion.15
  (125 shorter events, 8.6 us)
Async XLA Ops:
  6.5 67.8 %copy-start = (bf16[24,1024]{1,0:T(8,128)(2,1)S(1)}, bf16[24,1024]{1,0:T(8,128)(2,1)}, u32[]{:S(2)}) copy-start(bf16[24,1024]{1,0:T(8,128)(2,1)} %param.14) | copy-start | bytes 147460
  8.2 7.5 %copy-start.8 = (bf16[128,32]{0,1:T(8,128)(2,1)S(1)}, bf16[128,32]{0,1:T(8,128)(2,1)}, u32[]{:S(2)}) copy-start(bf16[128,32]{0,1:T(8,128)(2,1)} %param.21) | copy-start | bytes 24580
  8.2 239.5 %all-to-all-start = ((bf16[8,2,4096]{2,1,0:T(2,128)(2,1)}), bf16[8,2,4096]{2,1,0:T(2,128)(2,1)S(1)}, u32[]{:S(2)}, u32[]{:S(2)}) async-start(bf16[8,2,4096]{2,1,0:T(2,128)(2,1)} %reshape.149), calls=%async_computation | async-start | bytes 262144 | tf_op jit(solution)/shard_map/all_to_all | solution.py:102
  15.7 26.6 %copy-start.3 = (bf16[128,384]{1,0:T(8,128)(2,1)S(1)}, bf16[128,384]{1,0:T(8,128)(2,1)}, u32[]{:S(2)}) copy-start(bf16[128,384]{1,0:T(8,128)(2,1)} %param.16) | copy-start | bytes 294916
  15.7 251.3 %reduce-scatter.2.cloned.1.call-start = ((), (), s32[]{:S(2)}) async-start(), calls=%async_computation.2 | async-start | bytes 245760 | tf_op jit(solution)/shard_map/reduce_scatter | solution.py:31
  74.4 0.9 copy-start.4
  106.6 0.7 copy-start.10
  107.4 0.7 copy-start.11
  108.2 5.6 %copy-start.6 = (bf16[48,4,96]{2,1,0:T(4,128)(2,1)S(1)}, bf16[48,4,96]{2,1,0:T(4,128)(2,1)}, u32[]{:S(2)}) copy-start(bf16[48,4,96]{2,1,0:T(4,128)(2,1)} %param.18) | copy-start | bytes 110596
  113.8 31.4 %copy-start.1 = (bf16[96,672]{1,0:T(8,128)(2,1)}, bf16[96,672]{1,0:T(8,128)(2,1)S(1)}, u32[]{:S(2)}) copy-start(bf16[96,672]{1,0:T(8,128)(2,1)S(1)} %all_gather.27) | copy-start | bytes 387076
  145.2 0.8 copy-start.7
  146.0 30.9 %copy-start.12 = (s32[96]{0:T(128)S(1)}, s32[96]{0:T(128)}, u32[]{:S(2)}) copy-start(s32[96]{0:T(128)} %param.15) | copy-start | bytes 1156
  146.0 31.0 %slice-start = ((bf16[96,672]{1,0:T(8,128)(2,1)}), bf16[96,288]{1,0:T(8,128)(2,1)S(1)}, s32[]{:S(2)}) async-start(bf16[96,672]{1,0:T(8,128)(2,1)} %copy-done.1), calls=%async_computation.3 | async-start | bytes 147456 | tf_op jit(solution)/shard_map/slice | solution.py:121
  209.1 11.6 %copy-start.5 = (bf16[256,128]{1,0:T(8,128)(2,1)S(1)}, bf16[256,128]{1,0:T(8,128)(2,1)}, u32[]{:S(2)}) copy-start(bf16[256,128]{1,0:T(8,128)(2,1)} %param.24) | copy-start | bytes 196612
  248.5 19.5 %copy-start.9 = (f32[1024]{0:T(1024)S(1)}, f32[1024]{0:T(1024)}, u32[]{:S(2)}) copy-start(f32[1024]{0:T(1024)} %param.25) | copy-start | bytes 12292
  266.9 1.0 copy-start.2
Sparse Core Ops, SparseCore 0:
  249.5 17.3 reduce-scatter.1
